TPU v7x, 128 devices: a whole 4x4x4 slice. The times are simulated.
128 devices in a mesh: sp: 64 (over z, y, x), tp: 2 (over core).
Axes of the slice: x: 4, y: 4, z: 4, core: 2. Of those that a mesh axis runs over, the one named last changes fastest.
Arguments:
- stream: bfloat16 [16384, 2048], P(('sp', 'tp')), may hold values from -3 to 3
- query_narrow: bfloat16 [16384, 1024], P('sp', 'tp'), may hold values from -6 to 6
- key_narrow: bfloat16 [16384, 128], P('sp', 'tp'), may hold values from -6 to 6
- value_narrow: bfloat16 [16384, 128], P('sp', 'tp'), may hold values from -6 to 6
- query_broad: bfloat16 [16384, 1024], P('sp', 'tp'), may hold values from -6 to 6
- key_broad: bfloat16 [16384, 256], P('sp', 'tp'), may hold values from -6 to 6
- value_broad: bfloat16 [16384, 256], P('sp', 'tp'), may hold values from -6 to 6
- narrow_query_gain: float32 [64], replicated, may hold values from 1.5 to 9
- narrow_key_gain: float32 [64], replicated, may hold values from 1.5 to 9
- broad_query_gain: float32 [128], replicated, may hold values from 1.5 to 9
- broad_key_gain: float32 [128], replicated, may hold values from 1.5 to 9
- out_weight: bfloat16 [2048, 2048], replicated, may hold values from -0.125 to 0.125
- norm_gain: float32 [2048], replicated, may hold values from 0.1 to 1.9
- gate_weight: bfloat16 [64, 2048, 1024], P('sp', None, 'tp'), may hold values from -0.125 to 0.125
- up_weight: bfloat16 [64, 2048, 1024], P('sp', None, 'tp'), may hold values from -0.125 to 0.125
- down_weight: bfloat16 [64, 1024, 2048], P('sp', 'tp'), may hold values from -0.1875 to 0.1875
- route_ids: int32 [16384, 2], P(('sp', 'tp')), may hold values from 0 to 63, all different within a row; in each aligned block of 128 rows (0 to 127, 128 to 255, ...) at most 8 rows name the same one
- route_weights: float32 [16384, 2], P(('sp', 'tp')), may hold values from 0.1 to 1
Outputs:
- result: bfloat16 [16384, 2048], P(('sp', 'tp'))
Inputs may be any that keep to these rules, and one draw needn't show every extreme that they name: `route_ids`: in each aligned block of 128 rows no expert is named by more than 8 rows, a bound that some block reaches.
All inputs are finite; a program needn't handle non-finite values.
Results may differ from a plain program's by a relative error of at most 0.015.
The roundings to bfloat16 on the way count: a program that leaves them out, or rounds other values in their place, can miss the bound.
Values may be sent and summed in bfloat16 or wider, within the bound.
A program may use at most 128 MiB of HBM per device.

v0:
```python
import math
import jax
import jax.numpy as jnp
from jax import lax
from jax.sharding import PartitionSpec as P

HA = 16
DA = 64
DB = 128
GRID_W = 128
eps = 1e-06
theta = 10000.0


def cut_along(value, dim, size):
    before, after = (value.shape[:dim], value.shape[dim + 1 :])
    return jnp.moveaxis(value.reshape(*before, size, -1, *after), dim, 0)


def summed_on_arrival(value, axis, dim):
    size = lax.axis_size(axis)
    blocks = lax.all_to_all(cut_along(value, dim, size), axis, 0, 0, tiled=True)
    return jnp.sum(blocks.astype(jnp.float32), axis=0)


def joined_along(blocks, dim):
    shape = list(blocks.shape[1:])
    shape[dim] *= blocks.shape[0]
    return jnp.moveaxis(blocks, 0, dim).reshape(shape)


def copy_for_each(value, axis):
    size = lax.axis_size(axis)
    return lax.all_to_all(
        jnp.broadcast_to(value[None], (size, *value.shape)), axis, 0, 0, tiled=True
    )


def gather_directly(value, axis, dim):
    return joined_along(copy_for_each(value, axis), dim)


def rotate_grid(normed, positions):
    count, heads, dim = normed.shape
    freqs = dim // 4
    inverse = theta ** (-jnp.arange(freqs, dtype=jnp.float32) / freqs)
    rows = (positions // GRID_W).astype(jnp.float32)
    cols = (positions % GRID_W).astype(jnp.float32)
    angles = jnp.stack([rows[:, None] * inverse, cols[:, None] * inverse], axis=1)
    cosine = jnp.cos(angles)[:, None]
    sine = jnp.sin(angles)[:, None]
    split = normed.reshape(count, heads, 2, 2, freqs)
    first = split[..., 0, :]
    second = split[..., 1, :]
    turned = jnp.stack([first * cosine - second * sine, second * cosine + first * sine], axis=-2)
    return turned.reshape(count, heads, dim)


def prepare(raw, gain, dim, positions):
    count = raw.shape[0]
    values = raw.astype(jnp.float32).reshape(count, -1, dim)
    scaled = values * lax.rsqrt(jnp.mean(values * values, axis=-1, keepdims=True) + eps) * gain
    return rotate_grid(scaled, positions).reshape(count, -1).astype(jnp.bfloat16)


def arrange(queries, kv_width, dim):
    rows = queries.shape[0]
    heads_kv = kv_width // dim
    shaped = queries.reshape(rows, heads_kv, -1, dim)
    groups = shaped.shape[2]
    start = (
        jnp.full((heads_kv, groups, rows), -1e30, jnp.float32),
        jnp.zeros((heads_kv, groups, rows), jnp.float32),
        jnp.zeros((heads_kv, groups, rows, dim), jnp.float32),
    )
    return (shaped, start)


def attend_block(state, queries, keys, values):
    peak, total, summed = state
    dim = queries.shape[-1]
    scores = jnp.einsum(
        "qhgd,khd->hgqk", queries, keys, preferred_element_type=jnp.float32
    ) * dim ** (-0.5)
    fresh = jnp.maximum(peak, jnp.max(scores, axis=-1))
    weights = jnp.exp(scores - fresh[..., None])
    shrink = jnp.exp(peak - fresh)
    total = total * shrink + jnp.sum(weights, axis=-1)
    summed = summed * shrink[..., None] + jnp.einsum(
        "hgqk,khd->hgqd", weights.astype(jnp.bfloat16), values, preferred_element_type=jnp.float32
    )
    return (fresh, total, summed)


def sweep(state, keys, values, queries):
    rows = keys.shape[0]
    size = math.gcd(rows, 2048)
    count = rows // size

    def step(carry, block):
        return (attend_block(carry, queries, block[0], block[1]), None)

    blocks = (
        keys.reshape(count, size, keys.shape[1], keys.shape[2]),
        values.reshape(count, size, values.shape[1], values.shape[2]),
    )
    state, _ = lax.scan(step, state, blocks)
    return state


def make_fold(shaped_n, shaped_b, state, pieces):
    keys_n, values_n, keys_b, values_b = pieces
    rows = keys_n.shape[0]
    first = sweep(state[0], keys_n.reshape(rows, -1, DA), values_n.reshape(rows, -1, DA), shaped_n)
    second = sweep(state[1], keys_b.reshape(rows, -1, DB), values_b.reshape(rows, -1, DB), shaped_b)
    return (first, second)


def finish(state):
    peak, total, summed = state
    heads_out = summed / total[..., None]
    rows = heads_out.shape[2]
    return jnp.transpose(heads_out, (2, 0, 1, 3)).reshape(rows, -1).astype(jnp.bfloat16)


def local(
    stream,
    query_narrow,
    key_narrow,
    value_narrow,
    query_broad,
    key_broad,
    value_broad,
    narrow_query_gain,
    narrow_key_gain,
    broad_query_gain,
    broad_key_gain,
    out_weight,
    norm_gain,
    gate_weight,
    up_weight,
    down_weight,
    route_ids,
    route_weights,
):
    count = query_narrow.shape[0]
    positions = lax.axis_index("sp") * count + jnp.arange(count, dtype=jnp.int32)
    queries_n = prepare(query_narrow, narrow_query_gain, DA, positions)
    keys_n = prepare(key_narrow, narrow_key_gain, DA, positions)
    queries_b = prepare(query_broad, broad_query_gain, DB, positions)
    keys_b = prepare(key_broad, broad_key_gain, DB, positions)
    shaped_n, start_n = arrange(queries_n, keys_n.shape[1], DA)
    shaped_b, start_b = arrange(queries_b, keys_b.shape[1], DB)
    state = make_fold(
        shaped_n,
        shaped_b,
        (start_n, start_b),
        (
            lax.all_gather(keys_n, "sp", axis=0, tiled=True),
            lax.all_gather(value_narrow, "sp", axis=0, tiled=True),
            lax.all_gather(keys_b, "sp", axis=0, tiled=True),
            lax.all_gather(value_broad, "sp", axis=0, tiled=True),
        ),
    )
    heads_n = finish(state[0])
    heads_b = finish(state[1])
    width = heads_n.shape[1]
    place = lax.axis_index("tp")
    local_weight = jnp.concatenate(
        [
            lax.dynamic_slice_in_dim(out_weight, place * width, width, 0),
            lax.dynamic_slice_in_dim(out_weight, HA * DA + place * width, width, 0),
        ],
        axis=0,
    )
    local_heads = jnp.concatenate([heads_n, heads_b], axis=1)
    picked = local_heads
    mixed = summed_on_arrival(
        jnp.dot(picked, local_weight, preferred_element_type=jnp.float32).astype(jnp.bfloat16),
        "tp",
        0,
    )
    wide = (stream.astype(jnp.float32) + mixed).astype(jnp.bfloat16).astype(jnp.float32)
    normed = (
        wide * lax.rsqrt(jnp.mean(wide * wide, axis=-1, keepdims=True) + eps) * norm_gain
    ).astype(jnp.bfloat16)
    tokens_here, topk = route_ids.shape
    width_model = normed.shape[1]
    experts = lax.axis_size("sp")
    capacity = (2 * tokens_here * topk + experts - 1) // experts
    flat = route_ids.reshape(-1)
    hits = (flat[:, None] == jnp.arange(experts, dtype=jnp.int32)[None, :]).astype(jnp.int32)
    ranks = jnp.sum((jnp.cumsum(hits, axis=0) - 1) * hits, axis=1)
    slots = flat * capacity + ranks
    table = (jnp.arange(experts * capacity, dtype=jnp.int32)[:, None] == slots[None, :]).astype(
        jnp.bfloat16
    )
    table = jnp.sum(table.reshape(experts * capacity, tokens_here, topk), axis=2)
    sent = jnp.dot(table, normed, preferred_element_type=jnp.float32).astype(jnp.bfloat16)
    sent = sent.reshape(experts, capacity, width_model)
    piece = gather_directly(
        lax.all_to_all(sent, "sp", split_axis=0, concat_axis=0, tiled=True), "tp", 0
    )
    rows = piece.reshape(-1, piece.shape[-1])
    gate = jnp.dot(rows, gate_weight[0], preferred_element_type=jnp.float32)
    upper = jnp.dot(rows, up_weight[0], preferred_element_type=jnp.float32)
    hidden = (jax.nn.silu(gate) * upper).astype(jnp.bfloat16)
    partial_out = jnp.dot(hidden, down_weight[0], preferred_element_type=jnp.float32).astype(
        jnp.bfloat16
    )
    terms = lax.optimization_barrier(partial_out).astype(jnp.float32).reshape(piece.shape)
    summed = summed_on_arrival(terms.astype(jnp.bfloat16), "tp", 0).astype(jnp.bfloat16)
    back = lax.all_to_all(summed, "sp", split_axis=0, concat_axis=0, tiled=True)
    picked = jnp.take(back.reshape(experts * capacity, width_model), slots, axis=0)
    picked = picked.astype(jnp.float32).reshape(tokens_here, topk, width_model)
    routed = jnp.sum(picked * route_weights[..., None], axis=1)
    return (wide + routed).astype(jnp.bfloat16)


def solution(mesh):
    return jax.shard_map(
        local,
        mesh=mesh,
        in_specs=(
            P(("sp", "tp"), None),
            P("sp", "tp"),
            P("sp", "tp"),
            P("sp", "tp"),
            P("sp", "tp"),
            P("sp", "tp"),
            P("sp", "tp"),
            P(),
            P(),
            P(),
            P(),
            P(),
            P(),
            P("sp", None, "tp"),
            P("sp", None, "tp"),
            P("sp", "tp", None),
            P(("sp", "tp"), None),
            P(("sp", "tp"), None),
        ),
        out_specs=P(("sp", "tp"), None),
        check_vma=False,
    )
```

profile of v0, /device:TPU:0, one launch (start us, length us, event | category | flops | bytes accessed | tf_op | source)
XLA Modules:
  0.0 630.0 jit_solution(12985772197260481180)
XLA Ops:
  25.9 53.0 %all-gather.5.cloned.1.call-done = bf16[16384,64]{0,1:T(8,128)(2,1)} async-done(((bf16[256,64]{0,1:T(8,128)(2,1)}), bf16[16384,64]{0,1:T(8,128)(2,1)}) %all-gather.5.cloned.1.call-update) | async-done | bytes 2097168 | tf_op jit(solution)/shard_map/all_gather | solution.py:159
  84.2 63.0 %all-gather.7.cloned.1.call-done = bf16[16384,64]{0,1:T(8,128)(2,1)} async-done(((bf16[256,64]{0,1:T(8,128)(2,1)}), bf16[16384,64]{0,1:T(8,128)(2,1)}) %all-gather.7.cloned.1.call-update) | async-done | bytes 2097168 | tf_op jit(solution)/shard_map/all_gather | solution.py:160
  152.5 219.9 %while.30 = (s32[]{:T(128)}, f32[1,8,256]{2,1,0:T(8,128)S(1)}, f32[1,8,256]{2,1,0:T(8,128)S(1)}, f32[1,8,256,64]{2,3,1,0:T(8,128)}, bf16[8,2048,1,64]{1,3,2,0:T(...) while((s32[]{:T(128)}, f32[1,8,256]{2,1,0:T(8,128)S(1)}, ...), condition=%wide.region_5.6_spmd.clone, body=%wide.region_2.5_spmd.clone.sunk | while | flops 1107701760 | bytes 52298852 | solution.py:107
  152.8 9.0 %bitcast_reduce_fusion.6 = (f32[8,256]{1,0:T(8,128)S(1)}, f32[2048,256,8]{1,0,2:T(8,128)}) fusion(bf16[256,1,8,64]{0,3,2,1:T(8,128)(2,1)S(1)} %get-tuple-element.395, bf16[8,2048,1,64]{1,3,2,0:T(8,128)(2,1)} %get-tuple-element.394, s32[]{:T(128)} %get-tuple-element.381), kind=kOutput, calls=%fused_computation.2.clone.1 | convolution fusion | flops 545257472 | bytes 17310208 | tf_op jit(solution)/shard_map/while/body/eval_jaxpr/qhgd,khd->hgqk/dot_general | solution.py:82
  161.8 9.6 %fusion.116 = f32[1,8,256,64]{2,3,1,0:T(8,128)} fusion(f32[2048,256,8]{1,0,2:T(8,128)} %get-tuple-element.332, f32[8,256]{1,0:T(8,128)S(1)} %bitcast.237, f32[1,8,256,64]{2,3,1,0:T(8,128)} %get-tuple-element.384, bf16[8,2048,1,64]{1,3,2,0:T(8,128)(2,1)} %get-tuple-element.396, s32[]{:T(128)} %get-tuple-element.381, ...), kind=kOutput, calls=%fused_computation.9.clone.1 | convolution fusion | flops 549847040 | bytes 18104832 | tf_op jit(solution)/shard_map/while/body/eval_jaxpr/hgqk,khd->hgqd/dot_general | solution.py:89
  180.1 9.0 %bitcast_reduce_fusion.6 = (f32[8,256]{1,0:T(8,128)S(1)}, f32[2048,256,8]{1,0,2:T(8,128)}) fusion(bf16[256,1,8,64]{0,3,2,1:T(8,128)(2,1)S(1)} %get-tuple-element.395, bf16[8,2048,1,64]{1,3,2,0:T(8,128)(2,1)} %get-tuple-element.394, s32[]{:T(128)} %get-tuple-element.381), kind=kOutput, calls=%fused_computation.2.clone.1 | convolution fusion | flops 545257472 | bytes 17310208 | tf_op jit(solution)/shard_map/while/body/eval_jaxpr/qhgd,khd->hgqk/dot_general | solution.py:82
  189.1 9.7 %fusion.116 = f32[1,8,256,64]{2,3,1,0:T(8,128)} fusion(f32[2048,256,8]{1,0,2:T(8,128)} %get-tuple-element.332, f32[8,256]{1,0:T(8,128)S(1)} %bitcast.237, f32[1,8,256,64]{2,3,1,0:T(8,128)} %get-tuple-element.384, bf16[8,2048,1,64]{1,3,2,0:T(8,128)(2,1)} %get-tuple-element.396, s32[]{:T(128)} %get-tuple-element.381, ...), kind=kOutput, calls=%fused_computation.9.clone.1 | convolution fusion | flops 549847040 | bytes 18104832 | tf_op jit(solution)/shard_map/while/body/eval_jaxpr/hgqk,khd->hgqd/dot_general | solution.py:89
  207.8 9.0 %bitcast_reduce_fusion.6 = (f32[8,256]{1,0:T(8,128)S(1)}, f32[2048,256,8]{1,0,2:T(8,128)}) fusion(bf16[256,1,8,64]{0,3,2,1:T(8,128)(2,1)S(1)} %get-tuple-element.395, bf16[8,2048,1,64]{1,3,2,0:T(8,128)(2,1)} %get-tuple-element.394, s32[]{:T(128)} %get-tuple-element.381), kind=kOutput, calls=%fused_computation.2.clone.1 | convolution fusion | flops 545257472 | bytes 17310208 | tf_op jit(solution)/shard_map/while/body/eval_jaxpr/qhgd,khd->hgqk/dot_general | solution.py:82
  216.8 10.0 %fusion.116 = f32[1,8,256,64]{2,3,1,0:T(8,128)} fusion(f32[2048,256,8]{1,0,2:T(8,128)} %get-tuple-element.332, f32[8,256]{1,0:T(8,128)S(1)} %bitcast.237, f32[1,8,256,64]{2,3,1,0:T(8,128)} %get-tuple-element.384, bf16[8,2048,1,64]{1,3,2,0:T(8,128)(2,1)} %get-tuple-element.396, s32[]{:T(128)} %get-tuple-element.381, ...), kind=kOutput, calls=%fused_computation.9.clone.1 | convolution fusion | flops 549847040 | bytes 18104832 | tf_op jit(solution)/shard_map/while/body/eval_jaxpr/hgqk,khd->hgqd/dot_general | solution.py:89
  235.4 9.0 %bitcast_reduce_fusion.6 = (f32[8,256]{1,0:T(8,128)S(1)}, f32[2048,256,8]{1,0,2:T(8,128)}) fusion(bf16[256,1,8,64]{0,3,2,1:T(8,128)(2,1)S(1)} %get-tuple-element.395, bf16[8,2048,1,64]{1,3,2,0:T(8,128)(2,1)} %get-tuple-element.394, s32[]{:T(128)} %get-tuple-element.381), kind=kOutput, calls=%fused_computation.2.clone.1 | convolution fusion | flops 545257472 | bytes 17310208 | tf_op jit(solution)/shard_map/while/body/eval_jaxpr/qhgd,khd->hgqk/dot_general | solution.py:82
  244.5 9.7 %fusion.116 = f32[1,8,256,64]{2,3,1,0:T(8,128)} fusion(f32[2048,256,8]{1,0,2:T(8,128)} %get-tuple-element.332, f32[8,256]{1,0:T(8,128)S(1)} %bitcast.237, f32[1,8,256,64]{2,3,1,0:T(8,128)} %get-tuple-element.384, bf16[8,2048,1,64]{1,3,2,0:T(8,128)(2,1)} %get-tuple-element.396, s32[]{:T(128)} %get-tuple-element.381, ...), kind=kOutput, calls=%fused_computation.9.clone.1 | convolution fusion | flops 549847040 | bytes 18104832 | tf_op jit(solution)/shard_map/while/body/eval_jaxpr/hgqk,khd->hgqd/dot_general | solution.py:89
  262.8 9.1 %bitcast_reduce_fusion.6 = (f32[8,256]{1,0:T(8,128)S(1)}, f32[2048,256,8]{1,0,2:T(8,128)}) fusion(bf16[256,1,8,64]{0,3,2,1:T(8,128)(2,1)S(1)} %get-tuple-element.395, bf16[8,2048,1,64]{1,3,2,0:T(8,128)(2,1)} %get-tuple-element.394, s32[]{:T(128)} %get-tuple-element.381), kind=kOutput, calls=%fused_computation.2.clone.1 | convolution fusion | flops 545257472 | bytes 17310208 | tf_op jit(solution)/shard_map/while/body/eval_jaxpr/qhgd,khd->hgqk/dot_general | solution.py:82
  271.9 9.7 %fusion.116 = f32[1,8,256,64]{2,3,1,0:T(8,128)} fusion(f32[2048,256,8]{1,0,2:T(8,128)} %get-tuple-element.332, f32[8,256]{1,0:T(8,128)S(1)} %bitcast.237, f32[1,8,256,64]{2,3,1,0:T(8,128)} %get-tuple-element.384, bf16[8,2048,1,64]{1,3,2,0:T(8,128)(2,1)} %get-tuple-element.396, s32[]{:T(128)} %get-tuple-element.381, ...), kind=kOutput, calls=%fused_computation.9.clone.1 | convolution fusion | flops 549847040 | bytes 18104832 | tf_op jit(solution)/shard_map/while/body/eval_jaxpr/hgqk,khd->hgqd/dot_general | solution.py:89
  290.5 9.0 %bitcast_reduce_fusion.6 = (f32[8,256]{1,0:T(8,128)S(1)}, f32[2048,256,8]{1,0,2:T(8,128)}) fusion(bf16[256,1,8,64]{0,3,2,1:T(8,128)(2,1)S(1)} %get-tuple-element.395, bf16[8,2048,1,64]{1,3,2,0:T(8,128)(2,1)} %get-tuple-element.394, s32[]{:T(128)} %get-tuple-element.381), kind=kOutput, calls=%fused_computation.2.clone.1 | convolution fusion | flops 545257472 | bytes 17310208 | tf_op jit(solution)/shard_map/while/body/eval_jaxpr/qhgd,khd->hgqk/dot_general | solution.py:82
  299.6 9.7 %fusion.116 = f32[1,8,256,64]{2,3,1,0:T(8,128)} fusion(f32[2048,256,8]{1,0,2:T(8,128)} %get-tuple-element.332, f32[8,256]{1,0:T(8,128)S(1)} %bitcast.237, f32[1,8,256,64]{2,3,1,0:T(8,128)} %get-tuple-element.384, bf16[8,2048,1,64]{1,3,2,0:T(8,128)(2,1)} %get-tuple-element.396, s32[]{:T(128)} %get-tuple-element.381, ...), kind=kOutput, calls=%fused_computation.9.clone.1 | convolution fusion | flops 549847040 | bytes 18104832 | tf_op jit(solution)/shard_map/while/body/eval_jaxpr/hgqk,khd->hgqd/dot_general | solution.py:89
  317.8 9.0 %bitcast_reduce_fusion.6 = (f32[8,256]{1,0:T(8,128)S(1)}, f32[2048,256,8]{1,0,2:T(8,128)}) fusion(bf16[256,1,8,64]{0,3,2,1:T(8,128)(2,1)S(1)} %get-tuple-element.395, bf16[8,2048,1,64]{1,3,2,0:T(8,128)(2,1)} %get-tuple-element.394, s32[]{:T(128)} %get-tuple-element.381), kind=kOutput, calls=%fused_computation.2.clone.1 | convolution fusion | flops 545257472 | bytes 17310208 | tf_op jit(solution)/shard_map/while/body/eval_jaxpr/qhgd,khd->hgqk/dot_general | solution.py:82
  326.9 9.7 %fusion.116 = f32[1,8,256,64]{2,3,1,0:T(8,128)} fusion(f32[2048,256,8]{1,0,2:T(8,128)} %get-tuple-element.332, f32[8,256]{1,0:T(8,128)S(1)} %bitcast.237, f32[1,8,256,64]{2,3,1,0:T(8,128)} %get-tuple-element.384, bf16[8,2048,1,64]{1,3,2,0:T(8,128)(2,1)} %get-tuple-element.396, s32[]{:T(128)} %get-tuple-element.381, ...), kind=kOutput, calls=%fused_computation.9.clone.1 | convolution fusion | flops 549847040 | bytes 18104832 | tf_op jit(solution)/shard_map/while/body/eval_jaxpr/hgqk,khd->hgqd/dot_general | solution.py:89
  345.1 9.0 %bitcast_reduce_fusion.6 = (f32[8,256]{1,0:T(8,128)S(1)}, f32[2048,256,8]{1,0,2:T(8,128)}) fusion(bf16[256,1,8,64]{0,3,2,1:T(8,128)(2,1)S(1)} %get-tuple-element.395, bf16[8,2048,1,64]{1,3,2,0:T(8,128)(2,1)} %get-tuple-element.394, s32[]{:T(128)} %get-tuple-element.381), kind=kOutput, calls=%fused_computation.2.clone.1 | convolution fusion | flops 545257472 | bytes 17310208 | tf_op jit(solution)/shard_map/while/body/eval_jaxpr/qhgd,khd->hgqk/dot_general | solution.py:82
  354.2 9.7 %fusion.116 = f32[1,8,256,64]{2,3,1,0:T(8,128)} fusion(f32[2048,256,8]{1,0,2:T(8,128)} %get-tuple-element.332, f32[8,256]{1,0:T(8,128)S(1)} %bitcast.237, f32[1,8,256,64]{2,3,1,0:T(8,128)} %get-tuple-element.384, bf16[8,2048,1,64]{1,3,2,0:T(8,128)(2,1)} %get-tuple-element.396, s32[]{:T(128)} %get-tuple-element.381, ...), kind=kOutput, calls=%fused_computation.9.clone.1 | convolution fusion | flops 549847040 | bytes 18104832 | tf_op jit(solution)/shard_map/while/body/eval_jaxpr/hgqk,khd->hgqd/dot_general | solution.py:89
  380.6 103.4 %while.31 = (s32[]{:T(128)}, f32[1,4,256]{2,1,0:T(4,128)S(1)}, f32[1,4,256]{2,1,0:T(4,128)S(1)}, f32[1,4,256,128]{3,2,1,0:T(8,128)S(1)}, bf16[8,2048,1,128]{3,1,...) while((s32[]{:T(128)}, f32[1,4,256]{2,1,0:T(4,128)S(1)}, ...), condition=%wide.region_11.12_spmd.clone, body=%wide.region_8.11_spmd.clone.sunk | while | flops 1090918400 | bytes 61146240 | solution.py:107
  493.8 38.3 %all_to_all.26 = bf16[64,8,2048]{2,1,0:T(8,128)(2,1)S(1)} all-to-all(bf16[64,8,2048]{2,1,0:T(8,128)(2,1)S(1)} %fusion.48), channel_id=1, replica_groups=mesh['sp'=64,'tp'=2] {'sp'}, dimensions={0} | all-to-all | bytes 4194304 | tf_op jit(solution)/shard_map/all_to_all | solution.py:202
  545.8 10.0 %convolution_convert_fusion = bf16[1024,2048]{1,0:T(8,128)(2,1)} fusion(bf16[1,512,2048]{2,1,0:T(8,128)(2,1)S(1)} %copy-done, f32[1024,512]{1,0:T(8,128)} %fusion.53, bf16[1024,2048]{1,0:T(8,128)(2,1)} %bitcast.240, bf16[1,2048,512]{2,1,0:T(8,128)(2,1)} %param.35), kind=kOutput, calls=%fused_computation.53 | convolution fusion | flops 4300210176 | bytes 14680064 | tf_op jit(solution)/shard_map/dot_general | solution.py:208
  555.8 11.9 %all_to_all.28 = bf16[2,64,8,2048]{3,2,1,0:T(8,128)(2,1)} all-to-all(bf16[2,64,8,2048]{3,2,1,0:T(8,128)(2,1)} %bitcast.241), channel_id=1, replica_groups=mesh['sp'=64,'tp'=2] {'tp'}, dimensions={0} | all-to-all | bytes 8388608 | tf_op jit(solution)/shard_map/all_to_all | solution.py:22
  579.5 29.6 %all-to-all-done.4 = bf16[64,8,2048]{2,1,0:T(8,128)(2,1)} async-done(((bf16[64,8,2048]{2,1,0:T(8,128)(2,1)}), bf16[64,8,2048]{2,1,0:T(8,128)(2,1)}, u32[]{:S(2)}, u32[]{:S(2)}) %all-to-all-start.4) | async-done | bytes 2097184 | tf_op jit(solution)/shard_map/all_to_all | solution.py:213
  (211 shorter events, 259.1 us)
Async XLA Ops:
  6.5 539.2 %copy-start = (bf16[1,512,2048]{2,1,0:T(8,128)(2,1)S(1)}, bf16[1,512,2048]{2,1,0:T(8,128)(2,1)}, u32[]{:S(2)}) copy-start(bf16[1,512,2048]{2,1,0:T(8,128)(2,1)} %param.37) | copy-start | bytes 6291460
  6.5 13.6 %copy-start.6 = (s32[128,2]{0,1:T(2,128)S(1)}, s32[128,2]{0,1:T(2,128)}, u32[]{:S(2)}) copy-start(s32[128,2]{0,1:T(2,128)} %param.38) | copy-start | bytes 3076
  6.5 72.4 %all-gather.5.cloned.1.call-start = ((), (), s32[]{:S(2)}) async-start(), calls=%async_computation.5 | async-start | bytes 2129920 | tf_op jit(solution)/shard_map/all_gather | solution.py:159
  9.2 138.0 %all-gather.7.cloned.1.call-start = ((), (), s32[]{:S(2)}) async-start(), calls=%async_computation.6 | async-start | bytes 2129920 | tf_op jit(solution)/shard_map/all_gather | solution.py:160
  9.9 364.3 %all-gather.9.cloned.1.call-start = ((), (), s32[]{:S(2)}) async-start(), calls=%async_computation.7 | async-start | bytes 4259840 | tf_op jit(solution)/shard_map/all_gather | solution.py:161
  12.7 367.8 %all-gather.11.cloned.1.call-start = ((), (), s32[]{:S(2)}) async-start(), calls=%async_computation.8 | async-start | bytes 4259840 | tf_op jit(solution)/shard_map/all_gather | solution.py:162
  19.9 0.8 copy-start.4
  386.6 5.9 copy-start.1
  399.5 5.9 copy-start.1
  412.3 5.9 copy-start.1
  425.2 5.9 copy-start.1
  438.1 5.9 copy-start.1
  450.9 5.9 copy-start.1
  463.8 5.9 copy-start.1
  476.7 5.9 copy-start.1
  487.8 4.9 copy-start.3
  487.8 5.2 copy-start.8
  532.7 9.4 %copy-start.11 = (bf16[1,2048,512]{2,1,0:T(8,128)(2,1)S(1)}, bf16[1,2048,512]{2,1,0:T(8,128)(2,1)}, u32[]{:S(2)}) copy-start(bf16[1,2048,512]{2,1,0:T(8,128)(2,1)} %param.36) | copy-start | bytes 6291460
  540.1 2.0 copy-start.2
  567.7 11.3 %copy-start.7 = (s32[128,2]{0,1:T(2,128)S(1)}, s32[128,2]{0,1:T(2,128)}, u32[]{:S(2)}) copy-start(s32[128,2]{0,1:T(2,128)} %param.38) | copy-start | bytes 3076
  567.7 11.5 %copy-start.9 = (pred[128,2]{0,1:T(4,128)(4,1)S(1)}, pred[128,2]{0,1:T(4,128)(4,1)}, u32[]{:S(2)}) copy-start(pred[128,2]{0,1:T(4,128)(4,1)} %get-tuple-element.207) | copy-start | bytes 772
  567.7 11.7 %copy-start.10 = (f32[128,2]{0,1:T(2,128)S(1)}, f32[128,2]{0,1:T(2,128)}, u32[]{:S(2)}) copy-start(f32[128,2]{0,1:T(2,128)} %param.39) | copy-start | bytes 3076
  567.7 11.8 %copy-start.5 = (s32[256]{0:T(256)S(1)}, s32[256]{0:T(256)}, u32[]{:S(2)}) copy-start(s32[256]{0:T(256)} %copy-done.4) | copy-start | bytes 3076
  572.7 36.4 %all-to-all-start.4 = ((bf16[64,8,2048]{2,1,0:T(8,128)(2,1)}), bf16[64,8,2048]{2,1,0:T(8,128)(2,1)}, u32[]{:S(2)}, u32[]{:S(2)}) async-start(bf16[64,8,2048]{2,1,0:T(8,128)(2,1)} %reduce_sum.131), calls=%async_computation.4 | async-start | bytes 4194304 | tf_op jit(solution)/shard_map/all_to_all | solution.py:213
Sparse Core Ops, SparseCore 0:
  10.0 68.8 all-gather.4
  81.6 65.5 all-gather.6
  149.9 73.9 all-gather.8
  226.7 69.3 all-gather.10
where the time goes:
time: 638 us; the launch traced here: 630 us
  matrix products  254 us (40%)
  waiting for transfers between devices  147 us (23%)
  other arithmetic  101 us (16%)
  blocking collectives  62.3 us (10%)
  local copies, waits for them, and re-layouts  44.2 us (7%)
  between operations  13.7 us (2%)
    dot_general x16, matrix products, attend_block(): jnp.einsum('hgqk,khd->hgqd', weights.astype(jnp.bfloat16), values, prefer...  120 us
    dot_general x16, matrix products, attend_block(): jnp.einsum('qhgd,khd->hgqk', queries, keys, preferred_element_type=jnp.fl...  116 us
    reduce_sum x16, other arithmetic, attend_block(): total = total * shrink + jnp.sum(weights, axis=-1)  80.2 us
    all_gather x1, waiting for transfers between devices, local(): lax.all_gather(value_narrow, 'sp', axis=0, tiled=True)  63 us
    all_gather x1, waiting for transfers between devices, local(): lax.all_gather(keys_n, 'sp', axis=0, tiled=True)  53 us
    all_to_all x1, blocking collectives, local(): lax.all_to_all(sent, 'sp', split_axis=0, concat_axis=0, tiled=True)  38.3 us
    all_to_all x1, waiting for transfers between devices, local(): back = lax.all_to_all(summed, 'sp', split_axis=0, concat_axis=0, tiled=True)  29.6 us
    unnamed x33, local copies, waits for them, and re-layouts  23.1 us
  transfers between devices with their start and end apart: 5, of which 3 were waited for; matrix products, arithmetic and copies ran while one was open for 40% of the time, Pallas kernels for 0%

commit v1 on v0

--- a/solution.py
+++ b/solution.py
@@ -10,6 +10,11 @@
 GRID_W = 128
 eps = 1e-06
 theta = 10000.0
+
+
+def all_by_exchange(value, axis, dim):
+    sent = jnp.stack([value] * lax.axis_size(axis))
+    return jnp.concatenate(lax.all_to_all(sent, axis, 0, 0), axis=dim)
 
 
 def cut_along(value, dim, size):
@@ -157,7 +162,7 @@
         (start_n, start_b),
         (
             lax.all_gather(keys_n, "sp", axis=0, tiled=True),
-            lax.all_gather(value_narrow, "sp", axis=0, tiled=True),
+            all_by_exchange(value_narrow, "sp", 0),
             lax.all_gather(keys_b, "sp", axis=0, tiled=True),
             lax.all_gather(value_broad, "sp", axis=0, tiled=True),
         ),

time: 638 us -> 588 us (0.922)
  waiting for transfers between devices: 147 us -> 72.3 us
  starting transfers between devices: 6.3 us -> 18.1 us
  local copies, waits for them, and re-layouts: 44.2 us -> 51.8 us
    all_gather x1 -> x0, waiting for transfers between devices: 63 us -> none  [local(): lax.all_gather(value_narrow, 'sp', axis=0, tiled=True)]
    all_gather x1, waiting for transfers between devices: 53 us -> 26.2 us  [local(): lax.all_gather(keys_n, 'sp', axis=0, tiled=True)]
    all_to_all x0 -> x1, waiting for transfers between devices: none -> 15.7 us  [all_by_exchange(): return jnp.concatenate(lax.all_to_all(sent, axis, 0, 0), axis=dim)]
    all_to_all x0 -> x1, starting transfers between devices: none -> 11.8 us  [all_by_exchange(): return jnp.concatenate(lax.all_to_all(sent, axis, 0, 0), axis=dim)]
    another operation x1 -> x3, local copies, waits for them, and re-layouts: 0.02 us -> 6.56 us  [the longest x1 4.21 us: sweep(): values.reshape(count, size, values.shape[1], values.shape[2])]
    unnamed x33 -> x38, local copies, waits for them, and re-layouts: 23.1 us -> 20.3 us
  transfers between devices with their start and end apart: 5 -> 5, of which waited for: 3 -> 3; matrix products, arithmetic and copies ran while one was open for 40% -> 46% of each run, Pallas kernels for 0% -> 0%
where the time goes in v1:
time: 588 us; the launch traced here: 579 us
  matrix products  254 us (43%)
  other arithmetic  105 us (18%)
  waiting for transfers between devices  72.3 us (12%)
  blocking collectives  62.3 us (11%)
  local copies, waits for them, and re-layouts  51.8 us (9%)
  starting transfers between devices  18.1 us (3%)
  between operations  13.8 us (2%)
    dot_general x16, matrix products, attend_block(): jnp.einsum('hgqk,khd->hgqd', weights.astype(jnp.bfloat16), values, prefer...  120 us
    dot_general x16, matrix products, attend_block(): jnp.einsum('qhgd,khd->hgqk', queries, keys, preferred_element_type=jnp.fl...  116 us
    reduce_sum x16, other arithmetic, attend_block(): total = total * shrink + jnp.sum(weights, axis=-1)  80.2 us
    all_to_all x1, blocking collectives, local(): lax.all_to_all(sent, 'sp', split_axis=0, concat_axis=0, tiled=True)  38.3 us
    all_to_all x1, waiting for transfers between devices, local(): back = lax.all_to_all(summed, 'sp', split_axis=0, concat_axis=0, tiled=True)  29.6 us
    all_gather x1, waiting for transfers between devices, local(): lax.all_gather(keys_n, 'sp', axis=0, tiled=True)  26.2 us
    unnamed x38, local copies, waits for them, and re-layouts  20.3 us
    all_to_all x2, blocking collectives, summed_on_arrival(): blocks = lax.all_to_all(cut_along(value, dim, size), axis, 0, 0, tiled=True)  16.6 us
  transfers between devices with their start and end apart: 5, of which 3 were waited for; matrix products, arithmetic and copies ran while one was open for 46% of the time, Pallas kernels for 0%

profile of v1, /device:TPU:0, one launch (start us, length us, event | category | flops | bytes accessed | tf_op | source)
XLA Modules:
  0.0 578.9 jit_solution(17764624282338560809)
XLA Ops:
  15.6 11.8 %all-to-all-start = ((bf16[64,256,64]{1,2,0:T(8,128)(2,1)}), bf16[64,256,64]{1,2,0:T(8,128)(2,1)}, u32[]{:S(2)}, u32[]{:S(2)}) async-start(bf16[64,256,64]{1,2,0:T(8,128)(2,1)} %stack.36), calls=%async_computation | async-start | bytes 4194304 | tf_op jit(solution)/shard_map/all_to_all | solution.py:17
  41.7 15.7 %all-to-all-done = bf16[64,256,64]{1,2,0:T(8,128)(2,1)} async-done(((bf16[64,256,64]{1,2,0:T(8,128)(2,1)}), bf16[64,256,64]{1,2,0:T(8,128)(2,1)}, u32[]{:S(2)}, u32[]{:S(2)}) %all-to-all-start) | async-done | bytes 2097184 | tf_op jit(solution)/shard_map/all_to_all | solution.py:17
  69.9 26.2 %all-gather.4.cloned.1.call-done = bf16[16384,64]{0,1:T(8,128)(2,1)} async-done(((bf16[256,64]{0,1:T(8,128)(2,1)}), bf16[16384,64]{0,1:T(8,128)(2,1)}) %all-gather.4.cloned.1.call-update) | async-done | bytes 2097168 | tf_op jit(solution)/shard_map/all_gather | solution.py:164
  101.3 219.9 %while.30 = (s32[]{:T(128)}, f32[1,8,256]{2,1,0:T(8,128)S(1)}, f32[1,8,256]{2,1,0:T(8,128)S(1)}, f32[1,8,256,64]{2,3,1,0:T(8,128)}, bf16[8,2048,1,64]{1,3,2,0:T(...) while((s32[]{:T(128)}, f32[1,8,256]{2,1,0:T(8,128)S(1)}, ...), condition=%wide.region_5.6_spmd.clone, body=%wide.region_2.5_spmd.clone.sunk | while | flops 1107701760 | bytes 52298852 | solution.py:112
  101.6 9.0 %bitcast_reduce_fusion.6 = (f32[8,256]{1,0:T(8,128)S(1)}, f32[2048,256,8]{1,0,2:T(8,128)}) fusion(bf16[256,1,8,64]{0,3,2,1:T(8,128)(2,1)S(1)} %get-tuple-element.409, bf16[8,2048,1,64]{1,3,2,0:T(8,128)(2,1)} %get-tuple-element.408, s32[]{:T(128)} %get-tuple-element.395), kind=kOutput, calls=%fused_computation.2.clone.1 | convolution fusion | flops 545257472 | bytes 17310208 | tf_op jit(solution)/shard_map/while/body/eval_jaxpr/qhgd,khd->hgqk/dot_general | solution.py:87
  110.6 9.6 %fusion.116 = f32[1,8,256,64]{2,3,1,0:T(8,128)} fusion(f32[2048,256,8]{1,0,2:T(8,128)} %get-tuple-element.346, f32[8,256]{1,0:T(8,128)S(1)} %bitcast.233, f32[1,8,256,64]{2,3,1,0:T(8,128)} %get-tuple-element.398, bf16[8,2048,1,64]{1,3,2,0:T(8,128)(2,1)} %get-tuple-element.410, s32[]{:T(128)} %get-tuple-element.395, ...), kind=kOutput, calls=%fused_computation.9.clone.1 | convolution fusion | flops 549847040 | bytes 18104832 | tf_op jit(solution)/shard_map/while/body/eval_jaxpr/hgqk,khd->hgqd/dot_general | solution.py:94
  128.9 9.0 %bitcast_reduce_fusion.6 = (f32[8,256]{1,0:T(8,128)S(1)}, f32[2048,256,8]{1,0,2:T(8,128)}) fusion(bf16[256,1,8,64]{0,3,2,1:T(8,128)(2,1)S(1)} %get-tuple-element.409, bf16[8,2048,1,64]{1,3,2,0:T(8,128)(2,1)} %get-tuple-element.408, s32[]{:T(128)} %get-tuple-element.395), kind=kOutput, calls=%fused_computation.2.clone.1 | convolution fusion | flops 545257472 | bytes 17310208 | tf_op jit(solution)/shard_map/while/body/eval_jaxpr/qhgd,khd->hgqk/dot_general | solution.py:87
  137.9 9.7 %fusion.116 = f32[1,8,256,64]{2,3,1,0:T(8,128)} fusion(f32[2048,256,8]{1,0,2:T(8,128)} %get-tuple-element.346, f32[8,256]{1,0:T(8,128)S(1)} %bitcast.233, f32[1,8,256,64]{2,3,1,0:T(8,128)} %get-tuple-element.398, bf16[8,2048,1,64]{1,3,2,0:T(8,128)(2,1)} %get-tuple-element.410, s32[]{:T(128)} %get-tuple-element.395, ...), kind=kOutput, calls=%fused_computation.9.clone.1 | convolution fusion | flops 549847040 | bytes 18104832 | tf_op jit(solution)/shard_map/while/body/eval_jaxpr/hgqk,khd->hgqd/dot_general | solution.py:94
  156.6 9.0 %bitcast_reduce_fusion.6 = (f32[8,256]{1,0:T(8,128)S(1)}, f32[2048,256,8]{1,0,2:T(8,128)}) fusion(bf16[256,1,8,64]{0,3,2,1:T(8,128)(2,1)S(1)} %get-tuple-element.409, bf16[8,2048,1,64]{1,3,2,0:T(8,128)(2,1)} %get-tuple-element.408, s32[]{:T(128)} %get-tuple-element.395), kind=kOutput, calls=%fused_computation.2.clone.1 | convolution fusion | flops 545257472 | bytes 17310208 | tf_op jit(solution)/shard_map/while/body/eval_jaxpr/qhgd,khd->hgqk/dot_general | solution.py:87
  165.6 10.0 %fusion.116 = f32[1,8,256,64]{2,3,1,0:T(8,128)} fusion(f32[2048,256,8]{1,0,2:T(8,128)} %get-tuple-element.346, f32[8,256]{1,0:T(8,128)S(1)} %bitcast.233, f32[1,8,256,64]{2,3,1,0:T(8,128)} %get-tuple-element.398, bf16[8,2048,1,64]{1,3,2,0:T(8,128)(2,1)} %get-tuple-element.410, s32[]{:T(128)} %get-tuple-element.395, ...), kind=kOutput, calls=%fused_computation.9.clone.1 | convolution fusion | flops 549847040 | bytes 18104832 | tf_op jit(solution)/shard_map/while/body/eval_jaxpr/hgqk,khd->hgqd/dot_general | solution.py:94
  184.2 9.0 %bitcast_reduce_fusion.6 = (f32[8,256]{1,0:T(8,128)S(1)}, f32[2048,256,8]{1,0,2:T(8,128)}) fusion(bf16[256,1,8,64]{0,3,2,1:T(8,128)(2,1)S(1)} %get-tuple-element.409, bf16[8,2048,1,64]{1,3,2,0:T(8,128)(2,1)} %get-tuple-element.408, s32[]{:T(128)} %get-tuple-element.395), kind=kOutput, calls=%fused_computation.2.clone.1 | convolution fusion | flops 545257472 | bytes 17310208 | tf_op jit(solution)/shard_map/while/body/eval_jaxpr/qhgd,khd->hgqk/dot_general | solution.py:87
  193.3 9.7 %fusion.116 = f32[1,8,256,64]{2,3,1,0:T(8,128)} fusion(f32[2048,256,8]{1,0,2:T(8,128)} %get-tuple-element.346, f32[8,256]{1,0:T(8,128)S(1)} %bitcast.233, f32[1,8,256,64]{2,3,1,0:T(8,128)} %get-tuple-element.398, bf16[8,2048,1,64]{1,3,2,0:T(8,128)(2,1)} %get-tuple-element.410, s32[]{:T(128)} %get-tuple-element.395, ...), kind=kOutput, calls=%fused_computation.9.clone.1 | convolution fusion | flops 549847040 | bytes 18104832 | tf_op jit(solution)/shard_map/while/body/eval_jaxpr/hgqk,khd->hgqd/dot_general | solution.py:94
  211.6 9.1 %bitcast_reduce_fusion.6 = (f32[8,256]{1,0:T(8,128)S(1)}, f32[2048,256,8]{1,0,2:T(8,128)}) fusion(bf16[256,1,8,64]{0,3,2,1:T(8,128)(2,1)S(1)} %get-tuple-element.409, bf16[8,2048,1,64]{1,3,2,0:T(8,128)(2,1)} %get-tuple-element.408, s32[]{:T(128)} %get-tuple-element.395), kind=kOutput, calls=%fused_computation.2.clone.1 | convolution fusion | flops 545257472 | bytes 17310208 | tf_op jit(solution)/shard_map/while/body/eval_jaxpr/qhgd,khd->hgqk/dot_general | solution.py:87
  220.7 9.7 %fusion.116 = f32[1,8,256,64]{2,3,1,0:T(8,128)} fusion(f32[2048,256,8]{1,0,2:T(8,128)} %get-tuple-element.346, f32[8,256]{1,0:T(8,128)S(1)} %bitcast.233, f32[1,8,256,64]{2,3,1,0:T(8,128)} %get-tuple-element.398, bf16[8,2048,1,64]{1,3,2,0:T(8,128)(2,1)} %get-tuple-element.410, s32[]{:T(128)} %get-tuple-element.395, ...), kind=kOutput, calls=%fused_computation.9.clone.1 | convolution fusion | flops 549847040 | bytes 18104832 | tf_op jit(solution)/shard_map/while/body/eval_jaxpr/hgqk,khd->hgqd/dot_general | solution.py:94
  239.3 9.0 %bitcast_reduce_fusion.6 = (f32[8,256]{1,0:T(8,128)S(1)}, f32[2048,256,8]{1,0,2:T(8,128)}) fusion(bf16[256,1,8,64]{0,3,2,1:T(8,128)(2,1)S(1)} %get-tuple-element.409, bf16[8,2048,1,64]{1,3,2,0:T(8,128)(2,1)} %get-tuple-element.408, s32[]{:T(128)} %get-tuple-element.395), kind=kOutput, calls=%fused_computation.2.clone.1 | convolution fusion | flops 545257472 | bytes 17310208 | tf_op jit(solution)/shard_map/while/body/eval_jaxpr/qhgd,khd->hgqk/dot_general | solution.py:87
  248.4 9.7 %fusion.116 = f32[1,8,256,64]{2,3,1,0:T(8,128)} fusion(f32[2048,256,8]{1,0,2:T(8,128)} %get-tuple-element.346, f32[8,256]{1,0:T(8,128)S(1)} %bitcast.233, f32[1,8,256,64]{2,3,1,0:T(8,128)} %get-tuple-element.398, bf16[8,2048,1,64]{1,3,2,0:T(8,128)(2,1)} %get-tuple-element.410, s32[]{:T(128)} %get-tuple-element.395, ...), kind=kOutput, calls=%fused_computation.9.clone.1 | convolution fusion | flops 549847040 | bytes 18104832 | tf_op jit(solution)/shard_map/while/body/eval_jaxpr/hgqk,khd->hgqd/dot_general | solution.py:94
  266.6 9.0 %bitcast_reduce_fusion.6 = (f32[8,256]{1,0:T(8,128)S(1)}, f32[2048,256,8]{1,0,2:T(8,128)}) fusion(bf16[256,1,8,64]{0,3,2,1:T(8,128)(2,1)S(1)} %get-tuple-element.409, bf16[8,2048,1,64]{1,3,2,0:T(8,128)(2,1)} %get-tuple-element.408, s32[]{:T(128)} %get-tuple-element.395), kind=kOutput, calls=%fused_computation.2.clone.1 | convolution fusion | flops 545257472 | bytes 17310208 | tf_op jit(solution)/shard_map/while/body/eval_jaxpr/qhgd,khd->hgqk/dot_general | solution.py:87
  275.7 9.7 %fusion.116 = f32[1,8,256,64]{2,3,1,0:T(8,128)} fusion(f32[2048,256,8]{1,0,2:T(8,128)} %get-tuple-element.346, f32[8,256]{1,0:T(8,128)S(1)} %bitcast.233, f32[1,8,256,64]{2,3,1,0:T(8,128)} %get-tuple-element.398, bf16[8,2048,1,64]{1,3,2,0:T(8,128)(2,1)} %get-tuple-element.410, s32[]{:T(128)} %get-tuple-element.395, ...), kind=kOutput, calls=%fused_computation.9.clone.1 | convolution fusion | flops 549847040 | bytes 18104832 | tf_op jit(solution)/shard_map/while/body/eval_jaxpr/hgqk,khd->hgqd/dot_general | solution.py:94
  303.0 9.7 %fusion.116 = f32[1,8,256,64]{2,3,1,0:T(8,128)} fusion(f32[2048,256,8]{1,0,2:T(8,128)} %get-tuple-element.346, f32[8,256]{1,0:T(8,128)S(1)} %bitcast.233, f32[1,8,256,64]{2,3,1,0:T(8,128)} %get-tuple-element.398, bf16[8,2048,1,64]{1,3,2,0:T(8,128)(2,1)} %get-tuple-element.410, s32[]{:T(128)} %get-tuple-element.395, ...), kind=kOutput, calls=%fused_computation.9.clone.1 | convolution fusion | flops 549847040 | bytes 18104832 | tf_op jit(solution)/shard_map/while/body/eval_jaxpr/hgqk,khd->hgqd/dot_general | solution.py:94
  329.4 103.4 %while.31 = (s32[]{:T(128)}, f32[1,4,256]{2,1,0:T(4,128)S(1)}, f32[1,4,256]{2,1,0:T(4,128)S(1)}, f32[1,4,256,128]{3,2,1,0:T(8,128)S(1)}, bf16[8,2048,1,128]{3,1,...) while((s32[]{:T(128)}, f32[1,4,256]{2,1,0:T(4,128)S(1)}, ...), condition=%wide.region_11.12_spmd.clone, body=%wide.region_8.11_spmd.clone.sunk | while | flops 1090918400 | bytes 61146240 | solution.py:112
  442.6 38.3 %all_to_all.31 = bf16[64,8,2048]{2,1,0:T(8,128)(2,1)S(1)} all-to-all(bf16[64,8,2048]{2,1,0:T(8,128)(2,1)S(1)} %fusion.48), channel_id=1, replica_groups=mesh['sp'=64,'tp'=2] {'sp'}, dimensions={0} | all-to-all | bytes 4194304 | tf_op jit(solution)/shard_map/all_to_all | solution.py:207
  494.6 10.0 %convolution_convert_fusion = bf16[1024,2048]{1,0:T(8,128)(2,1)} fusion(bf16[1,512,2048]{2,1,0:T(8,128)(2,1)S(1)} %copy-done, f32[1024,512]{1,0:T(8,128)} %fusion.53, bf16[1024,2048]{1,0:T(8,128)(2,1)} %bitcast.236, bf16[1,2048,512]{2,1,0:T(8,128)(2,1)} %param.35), kind=kOutput, calls=%fused_computation.53 | convolution fusion | flops 4300210176 | bytes 14680064 | tf_op jit(solution)/shard_map/dot_general | solution.py:213
  504.6 11.9 %all_to_all.33 = bf16[2,64,8,2048]{3,2,1,0:T(8,128)(2,1)} all-to-all(bf16[2,64,8,2048]{3,2,1,0:T(8,128)(2,1)} %bitcast.237), channel_id=1, replica_groups=mesh['sp'=64,'tp'=2] {'tp'}, dimensions={0} | all-to-all | bytes 8388608 | tf_op jit(solution)/shard_map/all_to_all | solution.py:27
  528.3 29.6 %all-to-all-done.5 = bf16[64,8,2048]{2,1,0:T(8,128)(2,1)} async-done(((bf16[64,8,2048]{2,1,0:T(8,128)(2,1)}), bf16[64,8,2048]{2,1,0:T(8,128)(2,1)}, u32[]{:S(2)}, u32[]{:S(2)}) %all-to-all-start.5) | async-done | bytes 2097184 | tf_op jit(solution)/shard_map/all_to_all | solution.py:218
  (218 shorter events, 279.3 us)
Async XLA Ops:
  6.5 488.0 %copy-start = (bf16[1,512,2048]{2,1,0:T(8,128)(2,1)S(1)}, bf16[1,512,2048]{2,1,0:T(8,128)(2,1)}, u32[]{:S(2)}) copy-start(bf16[1,512,2048]{2,1,0:T(8,128)(2,1)} %param.37) | copy-start | bytes 6291460
  6.5 21.6 %copy-start.7 = (s32[128,2]{0,1:T(2,128)S(1)}, s32[128,2]{0,1:T(2,128)}, u32[]{:S(2)}) copy-start(s32[128,2]{0,1:T(2,128)} %param.38) | copy-start | bytes 3076
  6.5 23.2 %copy-start.4 = (bf16[256,512]{1,0:T(8,128)(2,1)S(1)}, bf16[256,512]{1,0:T(8,128)(2,1)}, u32[]{:S(2)}) copy-start(bf16[256,512]{1,0:T(8,128)(2,1)} %param.23) | copy-start | bytes 786436
  6.5 89.5 %all-gather.4.cloned.1.call-start = ((), (), s32[]{:S(2)}) async-start(), calls=%async_computation.6 | async-start | bytes 2129920 | tf_op jit(solution)/shard_map/all_gather | solution.py:164
  9.0 20.8 %copy-start.12 = (f32[64]{0:T(128)S(1)}, f32[64]{0:T(128)}, u32[]{:S(2)}) copy-start(f32[64]{0:T(128)} %param.29) | copy-start | bytes 772
  9.8 313.2 %all-gather.6.cloned.1.call-start = ((), (), s32[]{:S(2)}) async-start(), calls=%async_computation.7 | async-start | bytes 4259840 | tf_op jit(solution)/shard_map/all_gather | solution.py:166
  12.3 18.8 %copy-start.13 = (f32[128]{0:T(128)S(1)}, f32[128]{0:T(128)}, u32[]{:S(2)}) copy-start(f32[128]{0:T(128)} %param.31) | copy-start | bytes 1540
  15.6 41.9 %all-to-all-start = ((bf16[64,256,64]{1,2,0:T(8,128)(2,1)}), bf16[64,256,64]{1,2,0:T(8,128)(2,1)}, u32[]{:S(2)}, u32[]{:S(2)}) async-start(bf16[64,256,64]{1,2,0:T(8,128)(2,1)} %stack.36), calls=%async_computation | async-start | bytes 4194304 | tf_op jit(solution)/shard_map/all_to_all | solution.py:17
  27.4 302.0 %all-gather.8.cloned.1.call-start = ((), (), s32[]{:S(2)}) async-start(), calls=%async_computation.8 | async-start | bytes 4259840 | tf_op jit(solution)/shard_map/all_gather | solution.py:167
  34.9 6.8 %copy-start.5 = (s32[256]{0:T(256)}, s32[256]{0:T(256)S(1)}, u32[]{:S(2)}) copy-start(s32[256]{0:T(256)S(1)} %fusion.78) | copy-start | bytes 3076
  335.4 5.9 %copy-start.1 = (f32[2048,256,4]{1,0,2:T(8,128)S(1)}, f32[2048,256,4]{1,0,2:T(8,128)}, u32[]{:S(2)}) copy-start(f32[2048,256,4]{1,0,2:T(8,128)} %get-tuple-element.357) | copy-start | bytes 25165828 | tf_op jit(solution)/shard_map/while
  348.3 5.9 %copy-start.1 = (f32[2048,256,4]{1,0,2:T(8,128)S(1)}, f32[2048,256,4]{1,0,2:T(8,128)}, u32[]{:S(2)}) copy-start(f32[2048,256,4]{1,0,2:T(8,128)} %get-tuple-element.357) | copy-start | bytes 25165828 | tf_op jit(solution)/shard_map/while
  361.2 5.9 %copy-start.1 = (f32[2048,256,4]{1,0,2:T(8,128)S(1)}, f32[2048,256,4]{1,0,2:T(8,128)}, u32[]{:S(2)}) copy-start(f32[2048,256,4]{1,0,2:T(8,128)} %get-tuple-element.357) | copy-start | bytes 25165828 | tf_op jit(solution)/shard_map/while
  374.0 5.9 %copy-start.1 = (f32[2048,256,4]{1,0,2:T(8,128)S(1)}, f32[2048,256,4]{1,0,2:T(8,128)}, u32[]{:S(2)}) copy-start(f32[2048,256,4]{1,0,2:T(8,128)} %get-tuple-element.357) | copy-start | bytes 25165828 | tf_op jit(solution)/shard_map/while
  386.9 5.9 %copy-start.1 = (f32[2048,256,4]{1,0,2:T(8,128)S(1)}, f32[2048,256,4]{1,0,2:T(8,128)}, u32[]{:S(2)}) copy-start(f32[2048,256,4]{1,0,2:T(8,128)} %get-tuple-element.357) | copy-start | bytes 25165828 | tf_op jit(solution)/shard_map/while
  399.7 5.9 %copy-start.1 = (f32[2048,256,4]{1,0,2:T(8,128)S(1)}, f32[2048,256,4]{1,0,2:T(8,128)}, u32[]{:S(2)}) copy-start(f32[2048,256,4]{1,0,2:T(8,128)} %get-tuple-element.357) | copy-start | bytes 25165828 | tf_op jit(solution)/shard_map/while
  412.6 5.9 %copy-start.1 = (f32[2048,256,4]{1,0,2:T(8,128)S(1)}, f32[2048,256,4]{1,0,2:T(8,128)}, u32[]{:S(2)}) copy-start(f32[2048,256,4]{1,0,2:T(8,128)} %get-tuple-element.357) | copy-start | bytes 25165828 | tf_op jit(solution)/shard_map/while
  425.5 5.9 %copy-start.1 = (f32[2048,256,4]{1,0,2:T(8,128)S(1)}, f32[2048,256,4]{1,0,2:T(8,128)}, u32[]{:S(2)}) copy-start(f32[2048,256,4]{1,0,2:T(8,128)} %get-tuple-element.357) | copy-start | bytes 25165828 | tf_op jit(solution)/shard_map/while
  481.5 9.4 %copy-start.14 = (bf16[1,2048,512]{2,1,0:T(8,128)(2,1)S(1)}, bf16[1,2048,512]{2,1,0:T(8,128)(2,1)}, u32[]{:S(2)}) copy-start(bf16[1,2048,512]{2,1,0:T(8,128)(2,1)} %param.36) | copy-start | bytes 6291460
  516.5 11.3 %copy-start.8 = (s32[128,2]{0,1:T(2,128)S(1)}, s32[128,2]{0,1:T(2,128)}, u32[]{:S(2)}) copy-start(s32[128,2]{0,1:T(2,128)} %param.38) | copy-start | bytes 3076
  516.5 11.5 %copy-start.10 = (pred[128,2]{0,1:T(4,128)(4,1)S(1)}, pred[128,2]{0,1:T(4,128)(4,1)}, u32[]{:S(2)}) copy-start(pred[128,2]{0,1:T(4,128)(4,1)} %get-tuple-element.221) | copy-start | bytes 772
  516.5 11.7 %copy-start.11 = (f32[128,2]{0,1:T(2,128)S(1)}, f32[128,2]{0,1:T(2,128)}, u32[]{:S(2)}) copy-start(f32[128,2]{0,1:T(2,128)} %param.39) | copy-start | bytes 3076
  516.5 11.8 %copy-start.6 = (s32[256]{0:T(256)S(1)}, s32[256]{0:T(256)}, u32[]{:S(2)}) copy-start(s32[256]{0:T(256)} %copy-done.5) | copy-start | bytes 3076
  521.6 36.4 %all-to-all-start.5 = ((bf16[64,8,2048]{2,1,0:T(8,128)(2,1)}), bf16[64,8,2048]{2,1,0:T(8,128)(2,1)}, u32[]{:S(2)}, u32[]{:S(2)}) async-start(bf16[64,8,2048]{2,1,0:T(8,128)(2,1)} %reduce_sum.131), calls=%async_computation.5 | async-start | bytes 4194304 | tf_op jit(solution)/shard_map/all_to_all | solution.py:218
  (3 other events, 12.1 us)
Sparse Core Ops, SparseCore 0:
  10.0 85.9 all-gather.3
  98.8 73.9 all-gather.5
  175.7 69.3 all-gather.7
